TPU v7x, 256 devices: a whole 4x4x8 slice. The times are simulated.
256 devices in a mesh: ep: 64 (over z, y, core), tp: 4 (over x).
Axes of the slice: x: 4, y: 4, z: 8, core: 2. Of those that a mesh axis runs over, the one named last changes fastest.
Arguments:
- conv_value: bfloat16 [24576, 2048], P('ep', 'tp'), may hold values from -36 to 36
- conv_gate: bfloat16 [24576, 2048], P('ep', 'tp'), may hold values from -8 to 8
- conv_taps: bfloat16 [31, 2048], P(None, 'tp'), may hold values from -1 to 1
- conv_gain: float32 [2048], P('tp'), may hold values from 0.1 to 1.9
- conv_proj: bfloat16 [2048, 2048], P('tp'), may hold values from -0.125 to 0.125
- moe_tokens: bfloat16 [24576, 2048], P('ep'), may hold values from -6 to 6
- moe_gain: float32 [2048], replicated, may hold values from 0.1 to 1.9
- routes: int32 [24576, 2], P('ep'), may hold values from 0 to 63, all different within a row; in each aligned block of 384 rows (0 to 383, 384 to 767, ...) at most 18 rows name the same one
- route_weights: float32 [24576, 2], P('ep'), may hold values from 0.3 to 3
- expert_gate: bfloat16 [64, 2048, 1024], P('ep', None, 'tp'), may hold values from -0.125 to 0.125
- expert_up: bfloat16 [64, 2048, 1024], P('ep', None, 'tp'), may hold values from -0.125 to 0.125
- expert_down: bfloat16 [64, 1024, 2048], P('ep', 'tp'), may hold values from -0.1875 to 0.1875
- shared_gate: bfloat16 [2048, 256], replicated, may hold values from -0.125 to 0.125
- shared_up: bfloat16 [2048, 256], replicated, may hold values from -0.125 to 0.125
- shared_down: bfloat16 [256, 2048], P(None, 'tp'), may hold values from -0.375 to 0.375
Outputs:
- conv_result: bfloat16 [24576, 2048], P('ep', 'tp')
- moe_result: bfloat16 [24576, 2048], P('ep', 'tp')
Inputs may be any that keep to these rules, and one draw needn't show every extreme that they name: `routes`: each row names 2 different experts. Among the 384 rows of one index of ep (aligned blocks in order) no expert is named more than 18 times, and in some blocks one expert is named exactly 18 times.
All inputs are finite; a program needn't handle non-finite values.
Results may differ from a plain program's by a relative error of at most 0.01.
Values may be sent and summed in bfloat16 or wider, within the bound.
A program may use at most 64 MiB of HBM per device.

v0:
```python
import jax
import jax.numpy as jnp
from jax import lax
from jax.sharding import PartitionSpec as P

epsilon = 1e-05


def passed_along(value, axis, by):
    devices = lax.axis_size(axis)
    pairs = [(i, i + by) for i in range(devices) if 0 <= i + by < devices]
    return lax.ppermute(value, axis, pairs)


def total_of_pieces(value, axis):
    parts = lax.all_gather(value, axis)
    return parts.sum(axis=0)


def shared_hidden_rows(rows, shared_gate, shared_up):
    return (
        jax.nn.silu(jnp.dot(rows, shared_gate, preferred_element_type=jnp.float32))
        * jnp.dot(rows, shared_up, preferred_element_type=jnp.float32)
    ).astype(jnp.bfloat16)


def local(
    conv_value,
    conv_gate,
    conv_taps,
    conv_gain,
    conv_proj,
    moe_tokens,
    moe_gain,
    routes,
    route_weights,
    expert_gate,
    expert_up,
    expert_down,
    shared_gate,
    shared_up,
    shared_down,
):
    model_width = moe_tokens.shape[1]
    tok_rows = conv_value.shape[0]
    kernel = conv_taps.shape[0]
    gated_rows = (
        conv_value.astype(jnp.float32) * jax.nn.sigmoid(conv_gate.astype(jnp.float32))
    ).astype(jnp.bfloat16)
    previous = passed_along(gated_rows[tok_rows - (kernel - 1) :], "ep", 1)
    padded = jnp.concatenate([previous, gated_rows], axis=0).astype(jnp.float32)
    tap_weights = conv_taps.astype(jnp.float32)
    convolved = jnp.zeros(gated_rows.shape, jnp.float32)
    for offset in range(kernel):
        convolved = convolved + tap_weights[offset][None, :] * padded[offset : offset + tok_rows]
    total_sum, square_sum = (
        total_of_pieces(jnp.sum(convolved, axis=1), "tp"),
        total_of_pieces(jnp.sum(convolved * convolved, axis=1), "tp"),
    )
    average = total_sum / model_width
    variance = square_sum / model_width - average * average
    scaled = (
        (convolved - average[:, None]) * lax.rsqrt(variance + epsilon)[:, None] * conv_gain[None, :]
    )
    activated = jax.nn.silu(scaled).astype(jnp.bfloat16)
    conv_partial = jnp.dot(activated, conv_proj, preferred_element_type=jnp.float32)
    tokens = moe_tokens.astype(jnp.float32)
    token_mean = jnp.mean(tokens, axis=1, keepdims=True)
    centered = tokens - token_mean
    token_var = jnp.mean(centered * centered, axis=1, keepdims=True)
    normalized = (centered * lax.rsqrt(token_var + epsilon) * moe_gain[None, :]).astype(
        jnp.bfloat16
    )
    shared_hidden = shared_hidden_rows(normalized, shared_gate, shared_up)
    shared_part = jnp.dot(shared_hidden, shared_down, preferred_element_type=jnp.float32)
    experts = lax.axis_size("ep")
    top_count = routes.shape[1]
    capacity = 3 * tok_rows * top_count // (2 * experts)
    entries = tok_rows * top_count
    flat_routes = routes.reshape(-1)
    one_hot = (flat_routes[:, None] == jnp.arange(experts, dtype=jnp.int32)[None, :]).astype(
        jnp.int32
    )
    before = jnp.cumsum(one_hot, axis=0) - one_hot
    slot_rank = jnp.sum(before * one_hot, axis=1)
    slot_index = flat_routes * capacity + slot_rank
    source_row = (
        jnp.full((experts * capacity,), -1, jnp.int32)
        .at[slot_index]
        .set(jnp.arange(entries, dtype=jnp.int32))
    )
    filled = source_row >= 0
    token_index = jnp.where(filled, source_row // top_count, 0)
    outgoing = jnp.where(filled[:, None], normalized[token_index], jnp.zeros((), jnp.bfloat16))
    outgoing = outgoing.reshape(experts, capacity, model_width)
    quarter = model_width // lax.axis_size("tp")
    first_column = lax.axis_index("tp") * quarter
    column_block = lax.dynamic_slice_in_dim(outgoing, first_column, quarter, 2)
    arrived = lax.all_to_all(column_block, "ep", split_axis=0, concat_axis=0, tiled=True)
    arrived = lax.all_gather(arrived, "tp", axis=2, tiled=True)
    expert_input = arrived.reshape(experts * capacity, model_width)
    hidden = (
        jax.nn.silu(jnp.dot(expert_input, expert_gate[0], preferred_element_type=jnp.float32))
        * jnp.dot(expert_input, expert_up[0], preferred_element_type=jnp.float32)
    ).astype(jnp.bfloat16)
    expert_partial = jnp.dot(hidden, expert_down[0], preferred_element_type=jnp.float32)
    conv_sum, expert_sum = (
        lax.psum_scatter(
            conv_partial.astype(jnp.bfloat16), "tp", scatter_dimension=1, tiled=True
        ).astype(jnp.float32),
        lax.psum_scatter(
            expert_partial.astype(jnp.bfloat16), "tp", scatter_dimension=1, tiled=True
        ).astype(jnp.float32),
    )
    conv_result = conv_sum.astype(jnp.bfloat16)
    expert_rows = expert_sum.astype(jnp.bfloat16).reshape(experts, capacity, expert_sum.shape[1])
    returned = lax.all_to_all(expert_rows, "ep", split_axis=0, concat_axis=0, tiled=True)
    picked = returned.reshape(experts * capacity, returned.shape[2])[slot_index]
    picked = picked.astype(jnp.float32).reshape(tok_rows, top_count, returned.shape[2])
    moe_result = (shared_part + jnp.sum(route_weights[:, :, None] * picked, axis=1)).astype(
        jnp.bfloat16
    )
    return (conv_result, moe_result)


def solution(mesh):
    placed = (
        P("ep", "tp"),
        P("ep", "tp"),
        P(None, "tp"),
        P("tp"),
        P("tp", None),
        P("ep", None),
        P(),
        P("ep", None),
        P("ep", None),
        P("ep", None, "tp"),
        P("ep", None, "tp"),
        P("ep", "tp", None),
        P(),
        P(),
        P(None, "tp"),
    )
    return jax.shard_map(
        local, mesh=mesh, in_specs=placed, out_specs=(P("ep", "tp"), P("ep", "tp")), check_vma=False
    )
```

profile of v0, /device:TPU:1, one launch (start us, length us, event | category | flops | bytes accessed | tf_op | source)
XLA Modules:
  0.0 311.6 jit_solution(3662823600982574159)
XLA Ops:
  7.2 0.0 copy-start
  7.2 0.0 all-gather.6.cloned.1.call-start
  7.2 1.0 copy.25
  8.2 0.1 eq.29
  8.3 0.1 eq.25
  8.5 0.7 broadcast_multiply_fusion
  9.2 1.8 reduce-window.6
  11.0 0.3 slice_reduce_fusion
  11.3 0.1 copy.24
  11.4 0.2 mul.517
  11.6 0.1 fusion.60
  11.8 3.4 %scatter_custom_fusion = s32[1152]{0:T(1024)S(1)} fusion(s32[768]{0:T(1024)S(1)} %fusion.68, s32[768]{0:T(1024)S(1)} %iota.11, s32[]{:T(128)} %constant.26.clone.1), kind=kCustom, calls=%fused_computation.127 | custom fusion | bytes 4612 | tf_op jit(solution)/shard_map/scatter | solution.py:90
  15.2 0.0 copy-start.1
  15.2 0.0 copy-start.5
  15.2 1.8 convert_reduce_fusion
  17.1 0.0 copy-done.1
  17.1 0.6 fusion.2
  17.6 0.0 copy-done.5
  17.6 1.7 fusion.4
  19.3 12.3 %gather_fusion = bf16[1152,2048]{1,0:T(8,128)(2,1)} fusion(bf16[384,2048]{1,0:T(8,128)(2,1)} %fusion.4, s32[2048]{0:T(1024)S(1)} %pad_clamp_fusion), kind=kCustom, calls=%fused_computation | custom fusion | bytes 9441792 | tf_op jit(solution)/shard_map/gather | solution.py:94
  31.6 7.6 %gather.9 = bf16[64,18,2048]{2,1,0:T(8,128)(2,1)} reshape(bf16[1152,2048]{1,0:T(8,128)(2,1)} %gather_fusion) | data formatting | bytes 9437184 | tf_op jit(solution)/shard_map/gather | solution.py:94
  39.2 0.1 broadcast_in_dim.21
  39.3 1.8 dynamic-slice_select_fusion
  41.2 52.1 %all_to_all.10 = bf16[64,18,512]{2,1,0:T(8,128)(2,1)} all-to-all(bf16[64,18,512]{2,1,0:T(8,128)(2,1)S(1)} %dynamic-slice_select_fusion), channel_id=1, replica_groups=mesh['ep'=64,'tp'=4] {'ep'}, dimensions={0} | all-to-all | bytes 2359296 | tf_op jit(solution)/shard_map/all_to_all | solution.py:99
  93.3 0.0 all-gather.6.cloned.1.call-update
  93.3 0.2 reduce-scatter.5.cloned.1.call-start
  93.5 64.9 %all-gather.6.cloned.1.call-done = bf16[64,18,2048]{2,1,0:T(8,128)(2,1)} async-done(((bf16[64,18,512]{2,1,0:T(8,128)(2,1)}), bf16[64,18,2048]{2,1,0:T(8,128)(2,1)}) %all-gather.6.cloned.1.call-update) | async-done | bytes 4718608 | tf_op jit(solution)/shard_map/all_gather | solution.py:100
  158.5 7.8 %reshape.99 = bf16[1152,2048]{1,0:T(8,128)(2,1)} reshape(bf16[64,18,2048]{2,1,0:T(8,128)(2,1)} %all-gather.6.cloned.1.call-done) | data formatting | bytes 9437184 | tf_op jit(solution)/shard_map/reshape | solution.py:101
  166.2 5.1 %fusion.16 = f32[1152,256]{1,0:T(8,128)} fusion(bf16[1152,2048]{1,0:T(8,128)(2,1)} %reshape.99, bf16[1,2048,256]{2,1,0:T(8,128)(2,1)} %param.24), kind=kOutput, calls=%fused_computation.27 | convolution fusion | flops 1207959552 | bytes 6946816 | tf_op jit(solution)/shard_map/dot_general | solution.py:103
  171.3 10.3 %convolution_convert_fusion = bf16[1152,2048]{1,0:T(8,128)(2,1)} fusion(bf16[1152,2048]{1,0:T(8,128)(2,1)} %reshape.99, f32[1152,256]{1,0:T(8,128)} %fusion.16, bf16[1,256,2048]{2,1,0:T(8,128)(2,1)} %param.26, bf16[1,2048,256]{2,1,0:T(8,128)(2,1)} %param.25), kind=kOutput, calls=%fused_computation.3 | convolution fusion | flops 2420047872 | bytes 12713984 | tf_op jit(solution)/shard_map/dot_general | solution.py:106
  181.6 0.0 copy-start.2
  181.6 0.0 copy-start.3
  181.6 0.0 copy-start.4
  181.6 0.0 reduce-scatter.5.cloned.1.call-update
  181.6 0.0 reduce-scatter.3.cloned.1.call-start
  181.7 0.9 copy-done.2
  182.6 0.1 copy-done.3
  182.7 0.2 multiply_convert_fusion.1
  182.9 3.8 %collective-permute-start = (bf16[30,512]{1,0:T(8,128)(2,1)S(1)}, bf16[30,512]{1,0:T(8,128)(2,1)S(1)}, u32[]{:S(2)}, u32[]{:S(2)}) collective-permute-start(bf16[30,512]{1,0:T(8,128)(2,1)S(1)} %slice.265), channel_id=1, source_target_pairs={{0,4},{4,8},{8,12},{12,16},{16,20},{20,24},{24,28},{28,32},{32,36}... | collective-permute-start | bytes 92168 | tf_op jit(solution)/shard_map/ppermute | solution.py:12
  186.8 0.0 copy-done.4
  186.9 0.9 collective-permute-done
  187.8 0.1 maximum_convert_fusion
  187.9 0.0 copy-start.8
  187.9 3.8 %fusion.72 = (f32[384]{0:T(512)S(1)}, f32[384]{0:T(512)S(1)}, f32[384,512]{1,0:T(8,128)S(1)}) fusion(f32[414,512]{1,0:T(8,128)S(1)} %maximum_convert_fusion, f32[512]{0:T(512)S(1)} %bitcast.100, f32[512]{0:T(512)S(1)} %bitcast.99, f32[512]{0:T(512)S(1)} %bitcast.98, f32[512]{0:T(512)S(1)} %bitcast.97, f32[512]{0:T(512)S(1)} %bitcast.96, ...), kind=kLoop, calls=%fused_computation.138 | loop fusion | flops 12582144 | bytes 25232384 | tf_op jit(solution)/shard_map/reduce_sum | solution.py:57
  191.8 9.1 %all-gather.2 = f32[4,1,384]{2,1,0:T(1,128)S(1)} all-gather(f32[1,1,384]{2,1,0:T(1,128)S(1)} %reshape.130), channel_id=2, replica_groups=mesh['ep'=64,'tp'=4] {'tp'}, dimensions={0}, use_global_device_ids=true | all-gather | bytes 7680 | tf_op jit(solution)/shard_map/all_gather | solution.py:16
  200.9 9.6 %all-gather.3 = f32[4,1,384]{2,1,0:T(1,128)S(1)} all-gather(f32[1,1,384]{2,1,0:T(1,128)S(1)} %reshape.132), channel_id=3, replica_groups=mesh['ep'=64,'tp'=4] {'tp'}, dimensions={0}, use_global_device_ids=true | all-gather | bytes 7680 | tf_op jit(solution)/shard_map/all_gather | solution.py:16
  210.5 0.0 copy-done
  210.5 0.0 copy-done.8
  210.5 2.3 convolution_convert_fusion.1
  212.8 0.0 reduce-scatter.3.cloned.1.call-update
  212.9 23.5 %reduce-scatter.5.cloned.1.call-done = bf16[1152,512]{1,0:T(8,128)(2,1)} async-done(((bf16[1152,2048]{1,0:T(8,128)(2,1)}), bf16[1152,512]{1,0:T(8,128)(2,1)}) %reduce-scatter.5.cloned.1.call-update) | async-done | bytes 1179664 | tf_op jit(solution)/shard_map/reduce_scatter | solution.py:111
  236.4 3.0 reshape.100
  239.4 0.0 copy-start.6
  239.4 11.1 %all-to-all-start.1 = ((bf16[64,18,512]{2,1,0:T(8,128)(2,1)}), bf16[64,18,512]{2,1,0:T(8,128)(2,1)}, u32[]{:S(2)}, u32[]{:S(2)}) async-start(bf16[64,18,512]{2,1,0:T(8,128)(2,1)} %reshape.100), calls=%async_computation.3 | async-start | bytes 3145728 | tf_op jit(solution)/shard_map/all_to_all | solution.py:117
  250.5 0.0 copy-done.6
  250.5 0.1 copy.23
  250.7 3.1 fusion.76
  253.7 35.8 %all-to-all-done.1 = bf16[64,18,512]{2,1,0:T(8,128)(2,1)} async-done(((bf16[64,18,512]{2,1,0:T(8,128)(2,1)}), bf16[64,18,512]{2,1,0:T(8,128)(2,1)}, u32[]{:S(2)}, u32[]{:S(2)}) %all-to-all-start.1) | async-done | bytes 1179680 | tf_op jit(solution)/shard_map/all_to_all | solution.py:117
  289.5 2.3 reshape.101
  291.8 3.3 %gather_fusion.1 = bf16[768,512]{1,0:T(8,128)(2,1)} fusion(bf16[1152,512]{1,0:T(8,128)(2,1)S(1)} %reshape.101, s32[1024]{0:T(1024)S(1)} %pad_clamp_fusion.1), kind=kCustom, calls=%fused_computation.1 | custom fusion | bytes 1575936 | tf_op jit(solution)/shard_map/gather | solution.py:118
  295.1 3.0 reshape.102
  298.1 3.6 %multiply_reduce_fusion = f32[384,512]{1,0:T(8,128)S(1)} fusion(f32[384,2,512]{2,1,0:T(2,128)} %reshape.102, f32[384,2]{1,0:T(8,128)S(1)} %copy.23), kind=kLoop, calls=%fused_computation.15 | loop fusion | flops 589824 | bytes 2362368 | tf_op jit(solution)/shard_map/reduce_sum | solution.py:120
  301.7 0.0 copy-done.7
  301.7 3.4 %fusion.6 = bf16[384,512]{1,0:T(8,128)(2,1)} fusion(f32[384,512]{1,0:T(8,128)S(1)} %multiply_reduce_fusion, bf16[256,512]{1,0:T(8,128)(2,1)S(1)} %copy-done.7, bf16[384,2048]{1,0:T(8,128)(2,1)} %fusion.4, bf16[2048,256]{1,0:T(8,128)(2,1)} %param.28, f32[384,256]{1,0:T(8,128)} %fusion.76), kind=kOutput, calls=%fused_computation.17 | convolution fusion | flops 504299520 | bytes 4456448 | tf_op jit(solution)/shard_map/dot_general | solution.py:75
  (20 shorter events, 0.2 us)
Async XLA Ops:
  7.2 203.3 %copy-start = (bf16[512,2048]{1,0:T(8,128)(2,1)S(1)}, bf16[512,2048]{1,0:T(8,128)(2,1)}, u32[]{:S(2)}) copy-start(bf16[512,2048]{1,0:T(8,128)(2,1)} %param.19) | copy-start | bytes 6291460
  7.2 151.3 %all-gather.6.cloned.1.call-start = ((), (), s32[]{:S(2)}) async-start(), calls=%async_computation.5 | async-start | bytes 7864320 | tf_op jit(solution)/shard_map/all_gather | solution.py:100
  15.2 1.9 copy-start.1
  15.2 2.4 copy-start.5
  93.3 143.1 %reduce-scatter.5.cloned.1.call-start = ((), (), s32[]{:S(2)}) async-start(), calls=%async_computation.6 | async-start | bytes 5898240 | tf_op jit(solution)/shard_map/reduce_scatter | solution.py:111
  181.6 1.0 copy-start.2
  181.6 1.1 copy-start.3
  181.6 5.2 %copy-start.4 = (bf16[31,512]{1,0:T(8,128)(2,1)S(1)}, bf16[31,512]{1,0:T(8,128)(2,1)}, u32[]{:S(2)}) copy-start(bf16[31,512]{1,0:T(8,128)(2,1)} %param.17) | copy-start | bytes 95236
  181.6 123.5 %reduce-scatter.3.cloned.1.call-start = ((), (), s32[]{:S(2)}) async-start(), calls=%async_computation.4 | async-start | bytes 1966080 | tf_op jit(solution)/shard_map/reduce_scatter | solution.py:108
  182.9 4.9 %collective-permute-start = (bf16[30,512]{1,0:T(8,128)(2,1)S(1)}, bf16[30,512]{1,0:T(8,128)(2,1)S(1)}, u32[]{:S(2)}, u32[]{:S(2)}) collective-permute-start(bf16[30,512]{1,0:T(8,128)(2,1)S(1)} %slice.265), channel_id=1, source_target_pairs={{0,4},{4,8},{8,12},{12,16},{16,20},{20,24},{24,28},{28,32},{32,36}... | collective-permute-start | bytes 92168 | tf_op jit(solution)/shard_map/ppermute | solution.py:12
  187.9 22.6 %copy-start.8 = (f32[512]{0:T(512)S(1)}, f32[512]{0:T(512)}, u32[]{:S(2)}) copy-start(f32[512]{0:T(512)} %param.18) | copy-start | bytes 6148
  239.4 11.1 %copy-start.6 = (f32[384,2]{0,1:T(2,128)S(1)}, f32[384,2]{0,1:T(2,128)}, u32[]{:S(2)}) copy-start(f32[384,2]{0,1:T(2,128)} %param.23) | copy-start | bytes 9220
  239.4 50.1 %all-to-all-start.1 = ((bf16[64,18,512]{2,1,0:T(8,128)(2,1)}), bf16[64,18,512]{2,1,0:T(8,128)(2,1)}, u32[]{:S(2)}, u32[]{:S(2)}) async-start(bf16[64,18,512]{2,1,0:T(8,128)(2,1)} %reshape.100), calls=%async_computation.3 | async-start | bytes 3145728 | tf_op jit(solution)/shard_map/all_to_all | solution.py:117
  298.1 3.6 %copy-start.7 = (bf16[256,512]{1,0:T(8,128)(2,1)S(1)}, bf16[256,512]{1,0:T(8,128)(2,1)}, u32[]{:S(2)}) copy-start(bf16[256,512]{1,0:T(8,128)(2,1)} %param.29) | copy-start | bytes 786436
Sparse Core Ops, SparseCore 0:
  93.4 65.0 all-gather.5
  181.7 54.6 reduce-scatter.4
  239.5 27.0 reduce-scatter.2
where the time goes:
time: 313 us; the launch traced here: 312 us
  waiting for transfers between devices  125 us (40%)
  blocking collectives  70.7 us (23%)
  local copies, waits for them, and re-layouts  45.9 us (15%)
  matrix products  24.2 us (8%)
  other arithmetic  16.4 us (5%)
  starting transfers between devices  15.2 us (5%)
  between operations  14 us (4%)
    all_gather x1, waiting for transfers between devices, local(): arrived = lax.all_gather(arrived, 'tp', axis=2, tiled=True)  64.9 us
    all_to_all x1, blocking collectives, local(): lax.all_to_all(column_block, 'ep', split_axis=0, concat_axis=0, tiled=True)  52.1 us
    all_to_all x1, waiting for transfers between devices, local(): lax.all_to_all(expert_rows, 'ep', split_axis=0, concat_axis=0, tiled=True)  35.8 us
    reduce_scatter x1, waiting for transfers between devices, local(): lax.psum_scatter(expert_partial.astype(jnp.bfloat16), 'tp', scatter_dimen...  23.5 us
    gather x2, local copies, waits for them, and re-layouts, local(): normalized[token_index]  19.9 us
    all_gather x2, blocking collectives, total_of_pieces(): parts = lax.all_gather(value, axis)  18.6 us
    all_to_all x1, starting transfers between devices, local(): lax.all_to_all(expert_rows, 'ep', split_axis=0, concat_axis=0, tiled=True)  11.1 us
    dot_general x1, matrix products, local(): jnp.dot(hidden, expert_down[0], preferred_element_type=jnp.float32)  10.3 us
  transfers between devices with their start and end apart: 5, of which 4 were waited for; matrix products, arithmetic and copies ran while one was open for 9% of the time, Pallas kernels for 0%

commit v1 on v0

--- a/solution.py
+++ b/solution.py
@@ -97,7 +97,7 @@
     first_column = lax.axis_index("tp") * quarter
     column_block = lax.dynamic_slice_in_dim(outgoing, first_column, quarter, 2)
     arrived = lax.all_to_all(column_block, "ep", split_axis=0, concat_axis=0, tiled=True)
-    arrived = lax.all_gather(arrived, "tp", axis=2, tiled=True)
+    arrived = jnp.concatenate(lax.all_gather(arrived, "tp"), axis=2)
     expert_input = arrived.reshape(experts * capacity, model_width)
     hidden = (
         jax.nn.silu(jnp.dot(expert_input, expert_gate[0], preferred_element_type=jnp.float32))

time: 313 us -> 300 us (0.958)
  waiting for transfers between devices: 125 us -> 112 us
  local copies, waits for them, and re-layouts: 45.9 us -> 49.7 us
    all_gather x1, waiting for transfers between devices: 64.9 us -> 51.9 us  [local(): arrived = jnp.concatenate(lax.all_gather(arrived, 'tp'), axis=2)]
    reshape x1 -> x0, local copies, waits for them, and re-layouts: 7.77 us -> none  [local(): expert_input = arrived.reshape(experts * capacity, model_width)]
    all_gather x0 -> x1, local copies, waits for them, and re-layouts: none -> 5.98 us  [local(): arrived = jnp.concatenate(lax.all_gather(arrived, 'tp'), axis=2)]
    unnamed x22 -> x27, local copies, waits for them, and re-layouts: 2.18 us -> 6.34 us
  transfers between devices with their start and end apart: 5 -> 5, of which waited for: 4 -> 4; matrix products, arithmetic and copies ran while one was open for 9% -> 10% of each run, Pallas kernels for 0% -> 0%
where the time goes in v1:
time: 300 us; the launch traced here: 299 us
  waiting for transfers between devices  112 us (37%)
  blocking collectives  70.6 us (24%)
  local copies, waits for them, and re-layouts  49.7 us (17%)
  matrix products  21.5 us (7%)
  other arithmetic  16.4 us (5%)
  starting transfers between devices  15.4 us (5%)
  between operations  14.1 us (5%)
    all_to_all x1, blocking collectives, local(): lax.all_to_all(column_block, 'ep', split_axis=0, concat_axis=0, tiled=True)  52 us
    all_gather x1, waiting for transfers between devices, local(): arrived = jnp.concatenate(lax.all_gather(arrived, 'tp'), axis=2)  51.9 us
    all_to_all x1, waiting for transfers between devices, local(): lax.all_to_all(expert_rows, 'ep', split_axis=0, concat_axis=0, tiled=True)  35.8 us
    reduce_scatter x1, waiting for transfers between devices, local(): lax.psum_scatter(expert_partial.astype(jnp.bfloat16), 'tp', scatter_dimen...  23.3 us
    gather x2, local copies, waits for them, and re-layouts, local(): normalized[token_index]  19.9 us
    all_gather x2, blocking collectives, total_of_pieces(): parts = lax.all_gather(value, axis)  18.6 us
    all_to_all x1, starting transfers between devices, local(): lax.all_to_all(expert_rows, 'ep', split_axis=0, concat_axis=0, tiled=True)  11 us
    dot_general x1, matrix products, local(): jnp.dot(hidden, expert_down[0], preferred_element_type=jnp.float32)  10.3 us
  transfers between devices with their start and end apart: 5, of which 4 were waited for; matrix products, arithmetic and copies ran while one was open for 10% of the time, Pallas kernels for 0%

profile of v1, /device:TPU:1, one launch (start us, length us, event | category | flops | bytes accessed | tf_op | source)
XLA Modules:
  0.0 299.4 jit_solution(15770622330579259457)
XLA Ops:
  7.2 0.0 copy-start
  7.2 0.0 all-gather.7.cloned.1.call-start
  7.2 1.0 copy.26
  8.2 0.1 eq.29
  8.3 0.1 eq.25
  8.5 0.7 broadcast_multiply_fusion
  9.2 1.8 reduce-window.6
  11.0 0.3 slice_reduce_fusion
  11.3 0.1 copy.25
  11.4 0.2 mul.517
  11.6 0.1 fusion.60
  11.8 3.4 %scatter_custom_fusion = s32[1152]{0:T(1024)S(1)} fusion(s32[768]{0:T(1024)S(1)} %fusion.68, s32[768]{0:T(1024)S(1)} %iota.11, s32[]{:T(128)} %constant.26.clone.1), kind=kCustom, calls=%fused_computation.127 | custom fusion | bytes 4612 | tf_op jit(solution)/shard_map/scatter | solution.py:90
  15.2 0.0 copy-start.1
  15.2 0.0 copy-start.6
  15.2 1.8 convert_reduce_fusion
  17.1 0.0 copy-done.1
  17.1 0.6 fusion.2
  17.6 0.0 copy-done.6
  17.6 1.7 fusion.4
  19.3 12.3 %gather_fusion = bf16[1152,2048]{1,0:T(8,128)(2,1)} fusion(bf16[384,2048]{1,0:T(8,128)(2,1)} %fusion.4, s32[2048]{0:T(1024)S(1)} %pad_clamp_fusion), kind=kCustom, calls=%fused_computation | custom fusion | bytes 9441792 | tf_op jit(solution)/shard_map/gather | solution.py:94
  31.6 7.6 %gather.9 = bf16[64,18,2048]{2,1,0:T(8,128)(2,1)} reshape(bf16[1152,2048]{1,0:T(8,128)(2,1)} %gather_fusion) | data formatting | bytes 9437184 | tf_op jit(solution)/shard_map/gather | solution.py:94
  39.2 0.1 broadcast_in_dim.21
  39.3 1.8 dynamic-slice_select_fusion
  41.2 52.0 %all_to_all.10 = bf16[64,18,512]{2,1,0:T(8,128)(2,1)S(1)} all-to-all(bf16[64,18,512]{2,1,0:T(8,128)(2,1)S(1)} %dynamic-slice_select_fusion), channel_id=1, replica_groups=mesh['ep'=64,'tp'=4] {'ep'}, dimensions={0} | all-to-all | bytes 2359296 | tf_op jit(solution)/shard_map/all_to_all | solution.py:99
  93.2 1.4 copy.29
  94.6 0.0 all-gather.7.cloned.1.call-update
  94.6 0.2 reduce-scatter.5.cloned.1.call-start
  94.8 51.9 %all-gather.7.cloned.1.call-done = bf16[256,18,512]{2,0,1:T(8,128)(2,1)} async-done(((bf16[64,18,512]{2,0,1:T(8,128)(2,1)}), bf16[256,18,512]{2,0,1:T(8,128)(2,1)}) %all-gather.7.cloned.1.call-update) | async-done | bytes 4718608 | tf_op jit(solution)/shard_map/all_gather | solution.py:100
  146.7 6.0 %copy.30 = bf16[4,64,18,512]{3,0,2,1:T(4,128)(2,1)S(1)} copy(bf16[4,64,18,512]{3,1,0,2:T(8,128)(2,1)} %bitcast.75) | data formatting | bytes 9437184 | tf_op jit(solution)/shard_map/all_gather | solution.py:100
  152.7 0.0 copy-start.8
  152.7 2.0 copy.32
  154.7 0.0 copy-start.2
  154.7 2.2 copy-done.2
  156.9 0.0 copy-done.8
  156.9 2.4 fusion.16
  159.3 10.3 %convolution_convert_fusion = bf16[1152,2048]{1,0:T(8,128)(2,1)} fusion(bf16[1152,2048]{1,0:T(8,128)(2,1)} %bitcast.77, f32[1152,256]{1,0:T(8,128)} %fusion.16, bf16[1,256,2048]{2,1,0:T(8,128)(2,1)} %param.26, bf16[1,2048,256]{2,1,0:T(8,128)(2,1)} %param.25), kind=kOutput, calls=%fused_computation.3 | convolution fusion | flops 2420047872 | bytes 12713984 | tf_op jit(solution)/shard_map/dot_general | solution.py:106
  169.5 0.0 reduce-scatter.5.cloned.1.call-update
  169.6 0.0 reduce-scatter.3.cloned.1.call-start
  169.6 0.9 copy-done.3
  170.5 0.1 copy-done.4
  170.6 0.2 multiply_convert_fusion.1
  170.9 4.1 %collective-permute-start = (bf16[30,512]{1,0:T(8,128)(2,1)S(1)}, bf16[30,512]{1,0:T(8,128)(2,1)S(1)}, u32[]{:S(2)}, u32[]{:S(2)}) collective-permute-start(bf16[30,512]{1,0:T(8,128)(2,1)S(1)} %slice.265), channel_id=1, source_target_pairs={{0,4},{4,8},{8,12},{12,16},{16,20},{20,24},{24,28},{28,32},{32,36}... | collective-permute-start | bytes 92168 | tf_op jit(solution)/shard_map/ppermute | solution.py:12
  175.0 0.0 copy-done.5
  175.0 0.7 collective-permute-done
  175.7 0.1 maximum_convert_fusion
  175.9 0.0 copy-start.10
  175.9 3.8 %fusion.72 = (f32[384]{0:T(512)S(1)}, f32[384]{0:T(512)S(1)}, f32[384,512]{1,0:T(8,128)S(1)}) fusion(f32[414,512]{1,0:T(8,128)S(1)} %maximum_convert_fusion, f32[512]{0:T(512)S(1)} %bitcast.109, f32[512]{0:T(512)S(1)} %bitcast.108, f32[512]{0:T(512)S(1)} %bitcast.107, f32[512]{0:T(512)S(1)} %bitcast.106, f32[512]{0:T(512)S(1)} %bitcast.105, ...), kind=kLoop, calls=%fused_computation.138 | loop fusion | flops 12582144 | bytes 25232384 | tf_op jit(solution)/shard_map/reduce_sum | solution.py:57
  179.7 9.1 %all-gather.3 = f32[4,1,384]{2,1,0:T(1,128)S(1)} all-gather(f32[1,1,384]{2,1,0:T(1,128)S(1)} %reshape.131), channel_id=2, replica_groups=mesh['ep'=64,'tp'=4] {'tp'}, dimensions={0}, use_global_device_ids=true | all-gather | bytes 7680 | tf_op jit(solution)/shard_map/all_gather | solution.py:16
  188.8 9.6 %all-gather.4 = f32[4,1,384]{2,1,0:T(1,128)S(1)} all-gather(f32[1,1,384]{2,1,0:T(1,128)S(1)} %reshape.133), channel_id=3, replica_groups=mesh['ep'=64,'tp'=4] {'tp'}, dimensions={0}, use_global_device_ids=true | all-gather | bytes 7680 | tf_op jit(solution)/shard_map/all_gather | solution.py:16
  198.4 0.0 copy-done
  198.5 2.3 convolution_convert_fusion.1
  200.8 0.0 reduce-scatter.3.cloned.1.call-update
  200.8 23.3 %reduce-scatter.5.cloned.1.call-done = bf16[1152,512]{1,0:T(8,128)(2,1)} async-done(((bf16[1152,2048]{1,0:T(8,128)(2,1)}), bf16[1152,512]{1,0:T(8,128)(2,1)}) %reduce-scatter.5.cloned.1.call-update) | async-done | bytes 1179664 | tf_op jit(solution)/shard_map/reduce_scatter | solution.py:111
  224.1 3.0 %reshape.100 = bf16[64,18,512]{2,1,0:T(8,128)(2,1)} reshape(bf16[1152,512]{1,0:T(8,128)(2,1)} %reduce-scatter.5.cloned.1.call-done) | data formatting | bytes 2359296 | tf_op jit(solution)/shard_map/reshape | solution.py:116
  227.1 11.0 %all-to-all-start.1 = ((bf16[64,18,512]{2,1,0:T(8,128)(2,1)}), bf16[64,18,512]{2,1,0:T(8,128)(2,1)}, u32[]{:S(2)}, u32[]{:S(2)}) async-start(bf16[64,18,512]{2,1,0:T(8,128)(2,1)} %reshape.100), calls=%async_computation.3 | async-start | bytes 3145728 | tf_op jit(solution)/shard_map/all_to_all | solution.py:117
  238.2 0.0 copy-done.7
  238.2 0.1 copy.24
  238.4 3.1 %fusion.76 = f32[384,256]{1,0:T(8,128)} fusion(bf16[384,2048]{1,0:T(8,128)(2,1)} %fusion.4, bf16[2048,256]{1,0:T(8,128)(2,1)} %param.27), kind=kOutput, calls=%fused_computation.141 | convolution fusion | flops 402653184 | bytes 3014656 | tf_op jit(solution)/shard_map/dot_general | solution.py:22
  241.4 35.8 %all-to-all-done.1 = bf16[64,18,512]{2,1,0:T(8,128)(2,1)} async-done(((bf16[64,18,512]{2,1,0:T(8,128)(2,1)}), bf16[64,18,512]{2,1,0:T(8,128)(2,1)}, u32[]{:S(2)}, u32[]{:S(2)}) %all-to-all-start.1) | async-done | bytes 1179680 | tf_op jit(solution)/shard_map/all_to_all | solution.py:117
  277.2 2.3 reshape.101
  279.5 3.3 %gather_fusion.1 = bf16[768,512]{1,0:T(8,128)(2,1)} fusion(bf16[1152,512]{1,0:T(8,128)(2,1)S(1)} %reshape.101, s32[1024]{0:T(1024)S(1)} %pad_clamp_fusion.1), kind=kCustom, calls=%fused_computation.1 | custom fusion | bytes 1575936 | tf_op jit(solution)/shard_map/gather | solution.py:118
  282.8 3.0 reshape.102
  285.8 3.6 %multiply_reduce_fusion = f32[384,512]{1,0:T(8,128)S(1)} fusion(f32[384,2,512]{2,1,0:T(2,128)} %reshape.102, f32[384,2]{1,0:T(8,128)S(1)} %copy.24), kind=kLoop, calls=%fused_computation.15 | loop fusion | flops 589824 | bytes 2362368 | tf_op jit(solution)/shard_map/reduce_sum | solution.py:120
  289.4 3.4 %fusion.6 = bf16[384,512]{1,0:T(8,128)(2,1)} fusion(f32[384,512]{1,0:T(8,128)S(1)} %multiply_reduce_fusion, bf16[256,512]{1,0:T(8,128)(2,1)S(1)} %copy-done.9, bf16[384,2048]{1,0:T(8,128)(2,1)} %fusion.4, bf16[2048,256]{1,0:T(8,128)(2,1)} %param.28, f32[384,256]{1,0:T(8,128)} %fusion.76), kind=kOutput, calls=%fused_computation.17 | convolution fusion | flops 504299520 | bytes 4456448 | tf_op jit(solution)/shard_map/dot_general | solution.py:75
  (26 shorter events, 0.2 us)
Async XLA Ops:
  7.2 191.3 %copy-start = (bf16[512,2048]{1,0:T(8,128)(2,1)S(1)}, bf16[512,2048]{1,0:T(8,128)(2,1)}, u32[]{:S(2)}) copy-start(bf16[512,2048]{1,0:T(8,128)(2,1)} %param.19) | copy-start | bytes 6291460
  7.2 139.5 %all-gather.7.cloned.1.call-start = ((), (), s32[]{:S(2)}) async-start(), calls=%async_computation.6 | async-start | bytes 5898240 | tf_op jit(solution)/shard_map/all_gather | solution.py:100
  15.2 1.9 copy-start.1
  15.2 2.4 copy-start.6
  94.6 129.5 %reduce-scatter.5.cloned.1.call-start = ((), (), s32[]{:S(2)}) async-start(), calls=%async_computation.5 | async-start | bytes 5898240 | tf_op jit(solution)/shard_map/reduce_scatter | solution.py:111
  152.7 4.2 %copy-start.8 = (bf16[1,2048,256]{2,1,0:T(8,128)(2,1)S(1)}, bf16[1,2048,256]{2,1,0:T(8,128)(2,1)}, u32[]{:S(2)}) copy-start(bf16[1,2048,256]{2,1,0:T(8,128)(2,1)} %param.24) | copy-start | bytes 3145732
  154.7 2.2 copy-start.2
  169.5 1.0 copy-start.3
  169.5 1.1 copy-start.4
  169.5 5.4 %copy-start.5 = (bf16[31,512]{1,0:T(8,128)(2,1)S(1)}, bf16[31,512]{1,0:T(8,128)(2,1)}, u32[]{:S(2)}) copy-start(bf16[31,512]{1,0:T(8,128)(2,1)} %param.17) | copy-start | bytes 95236
  169.6 123.3 %reduce-scatter.3.cloned.1.call-start = ((), (), s32[]{:S(2)}) async-start(), calls=%async_computation.4 | async-start | bytes 1966080 | tf_op jit(solution)/shard_map/reduce_scatter | solution.py:108
  170.9 4.9 %collective-permute-start = (bf16[30,512]{1,0:T(8,128)(2,1)S(1)}, bf16[30,512]{1,0:T(8,128)(2,1)S(1)}, u32[]{:S(2)}, u32[]{:S(2)}) collective-permute-start(bf16[30,512]{1,0:T(8,128)(2,1)S(1)} %slice.265), channel_id=1, source_target_pairs={{0,4},{4,8},{8,12},{12,16},{16,20},{20,24},{24,28},{28,32},{32,36}... | collective-permute-start | bytes 92168 | tf_op jit(solution)/shard_map/ppermute | solution.py:12
  175.9 22.6 %copy-start.10 = (f32[512]{0:T(512)S(1)}, f32[512]{0:T(512)}, u32[]{:S(2)}) copy-start(f32[512]{0:T(512)} %param.18) | copy-start | bytes 6148
  227.1 11.1 %copy-start.7 = (f32[384,2]{0,1:T(2,128)S(1)}, f32[384,2]{0,1:T(2,128)}, u32[]{:S(2)}) copy-start(f32[384,2]{0,1:T(2,128)} %param.23) | copy-start | bytes 9220
  227.1 50.0 %all-to-all-start.1 = ((bf16[64,18,512]{2,1,0:T(8,128)(2,1)}), bf16[64,18,512]{2,1,0:T(8,128)(2,1)}, u32[]{:S(2)}, u32[]{:S(2)}) async-start(bf16[64,18,512]{2,1,0:T(8,128)(2,1)} %reshape.100), calls=%async_computation.3 | async-start | bytes 3145728 | tf_op jit(solution)/shard_map/all_to_all | solution.py:117
  285.8 3.6 %copy-start.9 = (bf16[256,512]{1,0:T(8,128)(2,1)S(1)}, bf16[256,512]{1,0:T(8,128)(2,1)}, u32[]{:S(2)}) copy-start(bf16[256,512]{1,0:T(8,128)(2,1)} %param.29) | copy-start | bytes 786436
Sparse Core Ops, SparseCore 0:
  94.7 51.9 all-gather.6
  169.7 54.3 reduce-scatter.4
  227.2 26.9 reduce-scatter.2
